TPU v7x, 512 devices: a 8x2x16 block of a 8x16x16 slice. The times are simulated.
512 devices in a mesh: grp: 2 (over y), kv: 16 (over z), tp: 16 (over x, core).
Axes of the slice: x: 8, y: 2, z: 16, core: 2. Of those that a mesh axis runs over, the one named last changes fastest.
The devices are a block of a 8x16x16 slice.
Arguments:
- tokens: bfloat16 [640, 4096], P('grp', ('kv', 'tp')), parts along dimension 0, may hold values from -65 to 65
- lengths: int32 [640], P(('grp', 'kv')), parts along dimension 0, may hold values from 1 to 16384, 1310720 in all
- memory: float32 [640, 16, 128, 128], P(('grp', 'kv'), 'tp'), parts along dimension 0, may hold values from -6 to 6
- norm_attn: bfloat16 [4096], P('kv'), may hold values from 0.099609375 to 1.8984375
- w_query: bfloat16 [4096, 2048], P('kv', 'tp'), may hold values from -0.09375 to 0.09375
- w_key: bfloat16 [4096, 2048], P('kv', 'tp'), may hold values from -0.09375 to 0.09375
- w_value: bfloat16 [4096, 2048], P('kv', 'tp'), may hold values from -0.09375 to 0.09375
- w_gate: bfloat16 [4096, 2048], P('kv', 'tp'), may hold values from -0.09375 to 0.09375
- head_gain: bfloat16 [2048], P('tp'), may hold values from 0.099609375 to 1.8984375
- w_out: bfloat16 [2048, 4096], P('tp', 'kv'), may hold values from -0.1875 to 0.1875
- norm_mlp: bfloat16 [4096], P('kv'), may hold values from 0.099609375 to 1.8984375
- w_gate_mlp: bfloat16 [4096, 14336], P('kv', 'tp'), may hold values from -0.09375 to 0.09375
- w_up: bfloat16 [4096, 14336], P('kv', 'tp'), may hold values from -0.09375 to 0.09375
- w_down: bfloat16 [14336, 4096], P('tp', 'kv'), may hold values from -0.0625 to 0.0625
Outputs:
- result: bfloat16 [640, 4096], P('grp', ('kv', 'tp')), parts along dimension 0
- new_memory: float32 [640, 16, 128, 128], P(('grp', 'kv'), 'tp'), parts along dimension 0
There are 2 independent parts, one for each index of `grp`. A program takes and returns all parts, laid end to end along the dimension named above; an argument that names none is the same for every part. Nothing has to cross between parts.
Inputs may be any that keep to these rules, and one draw needn't show every extreme that they name: Within each part along grp the lengths sum to 1310720 and the longest is exactly 16384.
All inputs are finite; a program needn't handle non-finite values. No bound on the sum of `lengths` on one device may be relied on, other than what follows from the above.
Results may differ from a plain program's by a relative error of at most 0.025.
Values may be sent and summed in bfloat16 or wider, within the bound.
No kernel may reach another device: no remote copies, remote signals or barrier semaphores. Data moves between devices by JAX's collectives and lax.ppermute only.
A program may use at most 64 MiB of HBM per device.

v0:
```python
import jax
import jax.numpy as jnp
from jax import lax
from jax.sharding import PartitionSpec as P

D = 4096
HEADS = 16
epsilon = 1e-06


def from_everyone(array, axis):
    copies = jnp.broadcast_to(array, (lax.axis_size(axis), *array.shape))
    return lax.all_to_all(copies, axis, split_axis=0, concat_axis=0, tiled=True)


def taken_together(array, axis):
    everything = from_everyone(array, axis)
    return jnp.sum(everything, axis=0)


def in_blocks(array, dim, size):
    lengths = array.shape
    pieces = array.reshape(*lengths[:dim], size, lengths[dim] // size, *lengths[dim + 1 :])
    return jnp.moveaxis(pieces, dim, 0)


def sum_at_owner(array, axis, dim):
    size = lax.axis_size(axis)
    pieces = lax.all_to_all(in_blocks(array, dim, size), axis, 0, 0, tiled=True)
    return jnp.sum(pieces.astype(jnp.float32), axis=0)


def rotate(values, position):
    half_width = values.shape[-1] // 2
    inverse = 10000.0 ** (-jnp.arange(half_width, dtype=jnp.float32) / half_width)
    angles = position[:, None] * inverse[None, :]
    cosine = jnp.cos(angles)[:, None, :]
    sine = jnp.sin(angles)[:, None, :]
    first = values[..., :half_width]
    second = values[..., half_width:]
    return jnp.concatenate(
        [first * cosine - second * sine, second * cosine + first * sine], axis=-1
    )


def head_decay(head_index):
    exponent = -5.0 - head_index.astype(jnp.float32) * (7.0 / max(HEADS - 1, 1))
    return 1.0 - jnp.exp2(exponent)


def retain(memory, queries, key_rows, value_rows, gate_rows, head_gain, decay_rate):
    new_memory = (
        decay_rate[None, :, None, None] * memory
        + key_rows[:, :, :, None] * value_rows[:, :, None, :]
    )
    readout = jnp.einsum(
        "bhd,bhde->bhe",
        queries * queries.shape[-1] ** (-0.5),
        new_memory,
        precision=lax.Precision.HIGHEST,
    )
    centred = readout - jnp.mean(readout, axis=-1, keepdims=True)
    normed = centred * lax.rsqrt(jnp.mean(centred * centred, axis=-1, keepdims=True) + epsilon)
    normed = normed.reshape(readout.shape[0], -1) * head_gain.astype(jnp.float32)
    return (new_memory, (normed * jax.nn.silu(gate_rows)).astype(jnp.bfloat16))


def per_device(
    tokens,
    lengths,
    memory,
    norm_attn,
    w_query,
    w_key,
    w_value,
    w_gate,
    head_gain,
    w_out,
    norm_mlp,
    w_gate_mlp,
    w_up,
    w_down,
):
    own_count = memory.shape[0]
    heads_local = memory.shape[1]
    head_size = memory.shape[2]
    width_local = w_query.shape[1]
    gathered = lax.all_gather(tokens, "tp", axis=1, tiled=True)
    tok_float = gathered.astype(jnp.float32)
    square_part = jnp.sum(tok_float * tok_float, axis=1)
    scaled = (tok_float * norm_attn.astype(jnp.float32)).astype(jnp.bfloat16)
    own_start = lax.axis_index("kv") * own_count
    square_total = taken_together(square_part, "kv")
    own_squares = lax.dynamic_slice_in_dim(square_total, own_start, own_count, 0)
    block_rows = scaled
    projected = sum_at_owner(
        jnp.concatenate(
            [
                jnp.dot(block_rows, weight, preferred_element_type=jnp.float32)
                for weight in (w_query, w_key, w_value, w_gate)
            ],
            axis=1,
        ).astype(jnp.bfloat16),
        "kv",
        0,
    )
    projected = projected * lax.rsqrt(own_squares / D + epsilon)[:, None]
    position = lengths.astype(jnp.float32)
    queries = rotate(
        projected[:, :width_local].reshape(own_count, heads_local, head_size), position
    )
    key_rows = rotate(
        projected[:, width_local : 2 * width_local].reshape(own_count, heads_local, head_size),
        position,
    )
    value_rows = projected[:, 2 * width_local : 3 * width_local].reshape(
        own_count, heads_local, head_size
    )
    gate_rows = projected[:, 3 * width_local :]
    decay_rate = head_decay(lax.axis_index("tp") * heads_local + jnp.arange(heads_local))
    new_memory, mixed = retain(
        memory, queries, key_rows, value_rows, gate_rows, head_gain, decay_rate
    )
    attn_part = jnp.dot(
        lax.all_gather(mixed, "kv", axis=0, tiled=True), w_out, preferred_element_type=jnp.float32
    )
    attn_total = sum_at_owner(attn_part.astype(jnp.bfloat16), "tp", 1)
    middle = (tokens.astype(jnp.float32) + attn_total).astype(jnp.bfloat16)
    mid_float = middle.astype(jnp.float32)
    gathered_mid = lax.all_gather(middle, "tp", axis=1, tiled=True)
    gathered_float = gathered_mid.astype(jnp.float32)
    mid_squares = jnp.sum(gathered_float * gathered_float, axis=1)
    scaled_mid = (gathered_float * norm_mlp.astype(jnp.float32)).astype(jnp.bfloat16)
    ff_local = w_up.shape[1]
    pieces = 1
    span = scaled_mid.shape[0] // pieces
    own_span = span // lax.axis_size("kv")
    span_start = lax.axis_index("kv") * own_span
    square_sums = taken_together(mid_squares, "kv")
    span_squares = lax.dynamic_slice_in_dim(square_sums, span_start, own_span, 0)
    block_rows = scaled_mid
    both_terms = lax.psum_scatter(
        jnp.concatenate(
            [
                jnp.dot(block_rows, w_gate_mlp, preferred_element_type=jnp.float32),
                jnp.dot(block_rows, w_up, preferred_element_type=jnp.float32),
            ],
            axis=1,
        ).astype(jnp.bfloat16),
        "kv",
        scatter_dimension=0,
        tiled=True,
    ).astype(jnp.float32)
    inv_mlp = lax.rsqrt(span_squares / D + epsilon)[:, None]
    gate_mlp = inv_mlp * both_terms[:, :ff_local]
    up_rows = inv_mlp * both_terms[:, ff_local:]
    hidden = (jax.nn.silu(gate_mlp) * up_rows).astype(jnp.bfloat16)
    partial_mlp = jnp.dot(
        lax.all_gather(hidden, "kv", axis=0, tiled=True), w_down, preferred_element_type=jnp.float32
    )
    results = sum_at_owner(partial_mlp.astype(jnp.bfloat16), "tp", 1)
    return ((mid_float + results).astype(jnp.bfloat16), new_memory)


def solution(mesh):
    in_specs = (
        P("grp", ("kv", "tp")),
        P(("grp", "kv")),
        P(("grp", "kv"), "tp", None, None),
        P("kv"),
        P("kv", "tp"),
        P("kv", "tp"),
        P("kv", "tp"),
        P("kv", "tp"),
        P("tp"),
        P("tp", "kv"),
        P("kv"),
        P("kv", "tp"),
        P("kv", "tp"),
        P("tp", "kv"),
    )
    out_specs = (P("grp", ("kv", "tp")), P(("grp", "kv"), "tp", None, None))
    return jax.shard_map(
        per_device, mesh=mesh, in_specs=in_specs, out_specs=out_specs, check_vma=False
    )
```

profile of v0, /device:TPU:65, one launch (start us, length us, event | category | flops | bytes accessed | tf_op | source)
XLA Modules:
  0.0 281.9 jit_solution(7506747860716999850)
XLA Ops:
  0.7 56.5 %all_gather.12 = bf16[320,256]{0,1:T(8,128)(2,1)S(1)} all-gather(bf16[320,16]{0,1:T(8,128)(2,1)} %param.14), channel_id=1, replica_groups=mesh['grp'=2,'kv'=16,'tp'=16] {'tp'}, dimensions={1}, use_global_device_ids=true | all-gather | bytes 174080 | tf_op jit(solution)/shard_map/all_gather | solution.py:88
  57.2 0.6 broadcast_in_dim.4
  57.8 7.1 %all-to-all-start.1 = ((f32[16,1,320]{2,1,0:T(1,128)}), f32[16,1,320]{2,1,0:T(1,128)S(1)}, u32[]{:S(2)}, u32[]{:S(2)}) async-start(f32[16,1,320]{2,1,0:T(1,128)} %broadcast_in_dim.4), calls=%async_computation.1 | async-start | bytes 49152 | tf_op jit(solution)/shard_map/all_to_all | solution.py:13
  64.9 0.7 convert_element_type.69
  65.6 1.1 convolution_convert_fusion.6
  66.8 1.2 convolution_convert_fusion.5
  68.7 0.8 pad_maximum_fusion.1
  69.5 6.7 %all-to-all-done.1 = f32[16,1,320]{2,1,0:T(1,128)S(1)} async-done(((f32[16,1,320]{2,1,0:T(1,128)}), f32[16,1,320]{2,1,0:T(1,128)S(1)}, u32[]{:S(2)}, u32[]{:S(2)}) %all-to-all-start.1) | async-done | bytes 20512 | tf_op jit(solution)/shard_map/all_to_all | solution.py:13
  76.2 4.7 %all-to-all-start = ((bf16[16,20,512]{2,1,0:T(8,128)(2,1)}), bf16[16,20,512]{2,1,0:T(8,128)(2,1)S(1)}, u32[]{:S(2)}, u32[]{:S(2)}) async-start(bf16[16,20,512]{2,1,0:T(8,128)(2,1)} %pad_maximum_fusion.1), calls=%async_computation | async-start | bytes 786432 | tf_op jit(solution)/shard_map/all_to_all | solution.py:29
  81.2 17.7 %all-to-all-done = bf16[16,20,512]{2,1,0:T(8,128)(2,1)S(1)} async-done(((bf16[16,20,512]{2,1,0:T(8,128)(2,1)}), bf16[16,20,512]{2,1,0:T(8,128)(2,1)S(1)}, u32[]{:S(2)}, u32[]{:S(2)}) %all-to-all-start) | async-done | bytes 327712 | tf_op jit(solution)/shard_map/all_to_all | solution.py:29
  99.3 0.4 multiply_add_fusion
  99.8 1.2 fusion.1
  101.4 26.0 %all-gather = bf16[16,20,128]{2,1,0:T(8,128)(2,1)S(1)} all-gather(bf16[1,20,128]{2,1,0:T(8,128)(2,1)S(1)} %fusion.28), channel_id=1, replica_groups=mesh['grp'=2,'kv'=16,'tp'=16] {'kv'}, dimensions={0}, use_global_device_ids=true | all-gather | bytes 87040 | tf_op jit(solution)/shard_map/all_gather | solution.py:125
  127.6 0.8 copy.23
  128.4 15.3 %all-to-all-start.2 = ((bf16[16,320,16]{1,2,0:T(8,128)(2,1)}), bf16[16,320,16]{1,2,0:T(8,128)(2,1)S(1)}, u32[]{:S(2)}, u32[]{:S(2)}) async-start(bf16[16,320,16]{1,2,0:T(8,128)(2,1)} %bitcast.10), calls=%async_computation.2 | async-start | bytes 393216 | tf_op jit(solution)/shard_map/all_to_all | solution.py:29
  143.7 1.3 dynamic-slice.4
  145.7 8.3 %all-to-all-done.2 = bf16[16,320,16]{1,2,0:T(8,128)(2,1)S(1)} async-done(((bf16[16,320,16]{1,2,0:T(8,128)(2,1)}), bf16[16,320,16]{1,2,0:T(8,128)(2,1)S(1)}, u32[]{:S(2)}, u32[]{:S(2)}) %all-to-all-start.2) | async-done | bytes 163872 | tf_op jit(solution)/shard_map/all_to_all | solution.py:29
  154.0 15.1 %all_gather.14 = bf16[320,256]{0,1:T(8,128)(2,1)S(1)} all-gather(bf16[320,16]{0,1:T(8,128)(2,1)S(1)} %add_convert_fusion.1), channel_id=1, replica_groups=mesh['grp'=2,'kv'=16,'tp'=16] {'tp'}, dimensions={1}, use_global_device_ids=true | all-gather | bytes 174080 | tf_op jit(solution)/shard_map/all_gather | solution.py:130
  169.1 0.6 broadcast_in_dim.5
  169.8 4.7 %all-to-all-start.3 = ((f32[16,1,320]{2,1,0:T(1,128)}), f32[16,1,320]{2,1,0:T(1,128)S(1)}, u32[]{:S(2)}, u32[]{:S(2)}) async-start(f32[16,1,320]{2,1,0:T(1,128)} %broadcast_in_dim.5), calls=%async_computation.3 | async-start | bytes 49152 | tf_op jit(solution)/shard_map/all_to_all | solution.py:13
  174.4 0.4 convolution_convert_fusion
  174.9 0.4 convolution_convert_fusion.1
  175.4 32.2 %fusion = bf16[24,1792]{1,0:T(8,128)(2,1)S(1)} fusion(bf16[320,1792]{1,0:T(8,128)(2,1)S(1)} %pad_maximum_fusion), kind=kCustom, calls=%all-reduce-scatter | all-reduce-scatter fusion | flops 688129 | bytes 1234944
  207.6 2.7 collective-permute-start.1
  210.3 2.9 %collective-permute-start = (bf16[24,1792]{1,0:T(8,128)(2,1)S(1)}, bf16[24,1792]{1,0:T(8,128)(2,1)S(1)}, u32[]{:S(2)}, u32[]{:S(2)}) collective-permute-start(bf16[24,1792]{1,0:T(8,128)(2,1)S(1)} %fusion), channel_id=1, source_target_pairs={{0,16},{16,32},{32,48},{48,64},{64,80},{80,96},{96,112},{112,128},... | collective-permute-start | bytes 258056
  213.3 5.5 %collective-permute-start.2 = (bf16[12,1792]{1,0:T(8,128)(2,1)S(1)}, bf16[12,1792]{1,0:T(8,128)(2,1)S(1)}, u32[]{:S(2)}, u32[]{:S(2)}) collective-permute-start(bf16[12,1792]{1,0:T(8,128)(2,1)S(1)} %slice.50), channel_id=1, source_target_pairs={{0,48},{16,64},{32,80},{48,96},{64,112},{80,128},{96,144},{112,160... | collective-permute-start | bytes 129032
  218.9 1.1 collective-permute-done.2
  220.1 0.6 concatenate.40
  220.8 28.5 %all-gather.1 = bf16[16,20,896]{2,1,0:T(8,128)(2,1)S(1)} all-gather(bf16[1,20,896]{2,1,0:T(8,128)(2,1)S(1)} %fusion.11), channel_id=1, replica_groups=mesh['grp'=2,'kv'=16,'tp'=16] {'kv'}, dimensions={0}, use_global_device_ids=true | all-gather | bytes 609280 | tf_op jit(solution)/shard_map/all_gather | solution.py:159
  249.5 0.3 convolution_convert_fusion.2
  250.0 31.3 %all_to_all.27 = bf16[16,320,16]{1,2,0:T(8,128)(2,1)S(1)} all-to-all(bf16[16,320,16]{1,2,0:T(8,128)(2,1)S(1)} %bitcast.47), channel_id=1, replica_groups=mesh['grp'=2,'kv'=16,'tp'=16] {'tp'}, dimensions={0} | all-to-all | bytes 327680 | tf_op jit(solution)/shard_map/all_to_all | solution.py:29
  281.3 0.6 add_convert_fusion
  (65 shorter events, 2.8 us)
Async XLA Ops:
  0.6 173.8 %copy-start = (bf16[256,896]{1,0:T(8,128)(2,1)S(1)}, bf16[256,896]{1,0:T(8,128)(2,1)}, u32[]{:S(2)}) copy-start(bf16[256,896]{1,0:T(8,128)(2,1)} %param.26) | copy-start | bytes 1376260
  0.6 67.3 %copy-start.6 = (bf16[256,128]{1,0:T(8,128)(2,1)S(1)}, bf16[256,128]{1,0:T(8,128)(2,1)}, u32[]{:S(2)}) copy-start(bf16[256,128]{1,0:T(8,128)(2,1)} %param.21) | copy-start | bytes 196612
  0.7 67.7 %copy-start.7 = (bf16[256,128]{1,0:T(8,128)(2,1)S(1)}, bf16[256,128]{1,0:T(8,128)(2,1)}, u32[]{:S(2)}) copy-start(bf16[256,128]{1,0:T(8,128)(2,1)} %param.18) | copy-start | bytes 196612
  57.8 18.4 %all-to-all-start.1 = ((f32[16,1,320]{2,1,0:T(1,128)}), f32[16,1,320]{2,1,0:T(1,128)S(1)}, u32[]{:S(2)}, u32[]{:S(2)}) async-start(f32[16,1,320]{2,1,0:T(1,128)} %broadcast_in_dim.4), calls=%async_computation.1 | async-start | bytes 49152 | tf_op jit(solution)/shard_map/all_to_all | solution.py:13
  68.0 13.1 %copy-start.9 = (s32[20]{0:T(128)S(1)}, s32[20]{0:T(128)}, u32[]{:S(2)}) copy-start(s32[20]{0:T(128)} %param.15) | copy-start | bytes 244
  68.0 13.1 %copy-start.10 = (bf16[128]{0:T(256)(128)(2,1)S(1)}, bf16[128]{0:T(256)(128)(2,1)}, u32[]{:S(2)}) copy-start(bf16[128]{0:T(256)(128)(2,1)} %param.22) | copy-start | bytes 772
  68.7 30.7 %copy-start.2 = (f32[20,1,128,128]{3,2,1,0:T(8,128)S(1)}, f32[20,1,128,128]{3,2,1,0:T(8,128)}, u32[]{:S(2)}) copy-start(f32[20,1,128,128]{3,2,1,0:T(8,128)} %param.16) | copy-start | bytes 3932164
  76.2 22.7 %all-to-all-start = ((bf16[16,20,512]{2,1,0:T(8,128)(2,1)}), bf16[16,20,512]{2,1,0:T(8,128)(2,1)S(1)}, u32[]{:S(2)}, u32[]{:S(2)}) async-start(bf16[16,20,512]{2,1,0:T(8,128)(2,1)} %pad_maximum_fusion.1), calls=%async_computation | async-start | bytes 786432 | tf_op jit(solution)/shard_map/all_to_all | solution.py:29
  99.8 28.7 %copy-start.1 = (f32[20,1,128,128]{3,2,1,0:T(8,128)}, f32[20,1,128,128]{3,2,1,0:T(8,128)S(1)}, u32[]{:S(2)}) copy-start(f32[20,1,128,128]{3,2,1,0:T(8,128)S(1)} %multiply_add_fusion) | copy-start | bytes 3932164
  99.8 27.6 %copy-start.5 = (bf16[128,256]{1,0:T(8,128)(2,1)S(1)}, bf16[128,256]{1,0:T(8,128)(2,1)}, u32[]{:S(2)}) copy-start(bf16[128,256]{1,0:T(8,128)(2,1)} %param.23) | copy-start | bytes 196612
  99.8 43.9 %copy-start.11 = (bf16[256]{0:T(256)(128)(2,1)S(1)}, bf16[256]{0:T(256)(128)(2,1)}, u32[]{:S(2)}) copy-start(bf16[256]{0:T(256)(128)(2,1)} %param.24) | copy-start | bytes 1540
  99.8 54.2 %copy-start.8 = (bf16[320,16]{0,1:T(8,128)(2,1)S(1)}, bf16[320,16]{0,1:T(8,128)(2,1)}, u32[]{:S(2)}) copy-start(bf16[320,16]{0,1:T(8,128)(2,1)} %param.14) | copy-start | bytes 30724
  127.6 47.3 %copy-start.3 = (bf16[256,896]{1,0:T(8,128)(2,1)S(1)}, bf16[256,896]{1,0:T(8,128)(2,1)}, u32[]{:S(2)}) copy-start(bf16[256,896]{1,0:T(8,128)(2,1)} %param.25) | copy-start | bytes 1376260
  128.4 25.5 %all-to-all-start.2 = ((bf16[16,320,16]{1,2,0:T(8,128)(2,1)}), bf16[16,320,16]{1,2,0:T(8,128)(2,1)S(1)}, u32[]{:S(2)}, u32[]{:S(2)}) async-start(bf16[16,320,16]{1,2,0:T(8,128)(2,1)} %bitcast.10), calls=%async_computation.2 | async-start | bytes 393216 | tf_op jit(solution)/shard_map/all_to_all | solution.py:29
  169.8 49.1 %all-to-all-start.3 = ((f32[16,1,320]{2,1,0:T(1,128)}), f32[16,1,320]{2,1,0:T(1,128)S(1)}, u32[]{:S(2)}, u32[]{:S(2)}) async-start(f32[16,1,320]{2,1,0:T(1,128)} %broadcast_in_dim.5), calls=%async_computation.3 | async-start | bytes 49152 | tf_op jit(solution)/shard_map/all_to_all | solution.py:13
  207.6 12.4 %collective-permute-start.1 = (bf16[24,1792]{1,0:T(8,128)(2,1)S(1)}, bf16[24,1792]{1,0:T(8,128)(2,1)S(1)}, u32[]{:S(2)}, u32[]{:S(2)}) collective-permute-start(bf16[24,1792]{1,0:T(8,128)(2,1)S(1)} %fusion), channel_id=1, source_target_pairs={{0,32},{16,48},{32,64},{48,80},{64,96},{80,112},{96,128},{112,144}... | collective-permute-start | bytes 258056
  210.3 9.7 %collective-permute-start = (bf16[24,1792]{1,0:T(8,128)(2,1)S(1)}, bf16[24,1792]{1,0:T(8,128)(2,1)S(1)}, u32[]{:S(2)}, u32[]{:S(2)}) collective-permute-start(bf16[24,1792]{1,0:T(8,128)(2,1)S(1)} %fusion), channel_id=1, source_target_pairs={{0,16},{16,32},{32,48},{48,64},{64,80},{80,96},{96,112},{112,128},... | collective-permute-start | bytes 258056
  213.3 6.8 %collective-permute-start.2 = (bf16[12,1792]{1,0:T(8,128)(2,1)S(1)}, bf16[12,1792]{1,0:T(8,128)(2,1)S(1)}, u32[]{:S(2)}, u32[]{:S(2)}) collective-permute-start(bf16[12,1792]{1,0:T(8,128)(2,1)S(1)} %slice.50), channel_id=1, source_target_pairs={{0,48},{16,64},{32,80},{48,96},{64,112},{80,128},{96,144},{112,160... | collective-permute-start | bytes 129032
  220.6 28.8 %copy-start.4 = (bf16[896,256]{1,0:T(8,128)(2,1)S(1)}, bf16[896,256]{1,0:T(8,128)(2,1)}, u32[]{:S(2)}) copy-start(bf16[896,256]{1,0:T(8,128)(2,1)} %param.27) | copy-start | bytes 1376260
where the time goes:
time: 283 us; the launch traced here: 282 us
  blocking collectives  190 us (67%)
  starting transfers between devices  42.9 us (15%)
  waiting for transfers between devices  33.8 us (12%)
  matrix products  5.51 us (2%)
  local copies, waits for them, and re-layouts  4.37 us (2%)
  other arithmetic  4 us (1%)
    all_gather x1, blocking collectives, per_device(): gathered = lax.all_gather(tokens, 'tp', axis=1, tiled=True)  56.5 us
    unnamed x1, blocking collectives  32.2 us
    all_to_all x1, blocking collectives, sum_at_owner(): pieces = lax.all_to_all(in_blocks(array, dim, size), axis, 0, 0, tiled=True)  31.3 us
    all_gather x1, blocking collectives, per_device(): lax.all_gather(hidden, 'kv', axis=0, tiled=True)  28.5 us
    all_gather x1, blocking collectives, per_device(): lax.all_gather(mixed, 'kv', axis=0, tiled=True)  26 us
    all_to_all x2, waiting for transfers between devices, sum_at_owner(): pieces = lax.all_to_all(in_blocks(array, dim, size), axis, 0, 0, tiled=True)  25.9 us
    all_to_all x2, starting transfers between devices, sum_at_owner(): pieces = lax.all_to_all(in_blocks(array, dim, size), axis, 0, 0, tiled=True)  20 us
    all_gather x1, blocking collectives, per_device(): gathered_mid = lax.all_gather(middle, 'tp', axis=1, tiled=True)  15.1 us
  transfers between devices with their start and end apart: 7, of which 4 were waited for; matrix products, arithmetic and copies ran while one was open for 14% of the time, Pallas kernels for 0%

commit v1 on v0

--- a/solution.py
+++ b/solution.py
@@ -6,6 +6,11 @@
 D = 4096
 HEADS = 16
 epsilon = 1e-06
+
+
+def exchange_gather(block, axis, dim):
+    repeated = jnp.stack([block] * lax.axis_size(axis))
+    return jnp.concatenate(lax.all_to_all(repeated, axis, 0, 0), axis=dim)
 
 
 def from_everyone(array, axis):
@@ -121,9 +126,7 @@
     new_memory, mixed = retain(
         memory, queries, key_rows, value_rows, gate_rows, head_gain, decay_rate
     )
-    attn_part = jnp.dot(
-        lax.all_gather(mixed, "kv", axis=0, tiled=True), w_out, preferred_element_type=jnp.float32
-    )
+    attn_part = jnp.dot(exchange_gather(mixed, "kv", 0), w_out, preferred_element_type=jnp.float32)
     attn_total = sum_at_owner(attn_part.astype(jnp.bfloat16), "tp", 1)
     middle = (tokens.astype(jnp.float32) + attn_total).astype(jnp.bfloat16)
     mid_float = middle.astype(jnp.float32)

time: 283 us -> 269 us (0.951)
  starting transfers between devices: 42.9 us -> 33.8 us
  blocking collectives: 190 us -> 185 us
    all_gather x1 -> x0, blocking collectives: 26 us -> none  [per_device(): lax.all_gather(mixed, 'kv', axis=0, tiled=True)]
    all_to_all x0 -> x1, blocking collectives: none -> 23 us  [exchange_gather(): return jnp.concatenate(lax.all_to_all(repeated, axis, 0, 0), axis=dim)]
    all_to_all x2, starting transfers between devices: 20 us -> 11.9 us  [sum_at_owner(): pieces = lax.all_to_all(in_blocks(array, dim, size), axis, 0, 0, tiled=True)]
  transfers between devices with their start and end apart: 7 -> 7, of which waited for: 4 -> 4; matrix products, arithmetic and copies ran while one was open for 14% -> 15% of each run, Pallas kernels for 0% -> 0%
where the time goes in v1:
time: 269 us
  blocking collectives  185 us (69%)
  starting transfers between devices  33.8 us (13%)
  waiting for transfers between devices  33.8 us (13%)
  matrix products  5.51 us (2%)
  local copies, waits for them, and re-layouts  4.39 us (2%)
  other arithmetic  4 us (1%)
    all_gather x1, blocking collectives, per_device(): gathered = lax.all_gather(tokens, 'tp', axis=1, tiled=True)  56.5 us
    unnamed x1, blocking collectives  32.1 us
    all_to_all x1, blocking collectives, sum_at_owner(): pieces = lax.all_to_all(in_blocks(array, dim, size), axis, 0, 0, tiled=True)  31.5 us
    all_gather x1, blocking collectives, per_device(): lax.all_gather(hidden, 'kv', axis=0, tiled=True)  27.3 us
    all_to_all x2, waiting for transfers between devices, sum_at_owner(): pieces = lax.all_to_all(in_blocks(array, dim, size), axis, 0, 0, tiled=True)  25.9 us
    all_to_all x1, blocking collectives, exchange_gather(): return jnp.concatenate(lax.all_to_all(repeated, axis, 0, 0), axis=dim)  23 us
    all_gather x1, blocking collectives, per_device(): gathered_mid = lax.all_gather(middle, 'tp', axis=1, tiled=True)  15.1 us
    all_to_all x2, starting transfers between devices, sum_at_owner(): pieces = lax.all_to_all(in_blocks(array, dim, size), axis, 0, 0, tiled=True)  11.9 us
  transfers between devices with their start and end apart: 7, of which 4 were waited for; matrix products, arithmetic and copies ran while one was open for 15% of the time, Pallas kernels for 0%

profile of v1, /device:TPU:65, one launch (start us, length us, event | category | flops | bytes accessed | tf_op | source)
XLA Modules:
  0.0 268.7 jit_solution(4043496603325899727)
XLA Ops:
  0.7 56.5 %all_gather.9 = bf16[320,256]{0,1:T(8,128)(2,1)S(1)} all-gather(bf16[320,16]{0,1:T(8,128)(2,1)} %param.14), channel_id=1, replica_groups=mesh['grp'=2,'kv'=16,'tp'=16] {'tp'}, dimensions={1}, use_global_device_ids=true | all-gather | bytes 174080 | tf_op jit(solution)/shard_map/all_gather | solution.py:93
  57.2 0.6 broadcast_in_dim.4
  57.8 7.1 %all-to-all-start.1 = ((f32[16,1,320]{2,1,0:T(1,128)}), f32[16,1,320]{2,1,0:T(1,128)S(1)}, u32[]{:S(2)}, u32[]{:S(2)}) async-start(f32[16,1,320]{2,1,0:T(1,128)} %broadcast_in_dim.4), calls=%async_computation.1 | async-start | bytes 49152 | tf_op jit(solution)/shard_map/all_to_all | solution.py:18
  64.9 0.7 convert_element_type.69
  65.6 1.1 convolution_convert_fusion.6
  66.8 1.2 convolution_convert_fusion.5
  68.7 0.8 pad_maximum_fusion.1
  69.5 6.7 %all-to-all-done.1 = f32[16,1,320]{2,1,0:T(1,128)S(1)} async-done(((f32[16,1,320]{2,1,0:T(1,128)}), f32[16,1,320]{2,1,0:T(1,128)S(1)}, u32[]{:S(2)}, u32[]{:S(2)}) %all-to-all-start.1) | async-done | bytes 20512 | tf_op jit(solution)/shard_map/all_to_all | solution.py:18
  76.2 4.7 %all-to-all-start = ((bf16[16,20,512]{2,1,0:T(8,128)(2,1)}), bf16[16,20,512]{2,1,0:T(8,128)(2,1)S(1)}, u32[]{:S(2)}, u32[]{:S(2)}) async-start(bf16[16,20,512]{2,1,0:T(8,128)(2,1)} %pad_maximum_fusion.1), calls=%async_computation | async-start | bytes 786432 | tf_op jit(solution)/shard_map/all_to_all | solution.py:34
  81.2 17.7 %all-to-all-done = bf16[16,20,512]{2,1,0:T(8,128)(2,1)S(1)} async-done(((bf16[16,20,512]{2,1,0:T(8,128)(2,1)}), bf16[16,20,512]{2,1,0:T(8,128)(2,1)S(1)}, u32[]{:S(2)}, u32[]{:S(2)}) %all-to-all-start) | async-done | bytes 327712 | tf_op jit(solution)/shard_map/all_to_all | solution.py:34
  99.3 0.4 multiply_add_fusion
  99.8 1.2 fusion.1
  101.4 23.0 %all_to_all.32 = bf16[16,20,128]{2,1,0:T(8,128)(2,1)S(1)} all-to-all(bf16[16,20,128]{2,1,0:T(8,128)(2,1)S(1)} %stack.2), channel_id=1, replica_groups=mesh['grp'=2,'kv'=16,'tp'=16] {'kv'}, dimensions={0} | all-to-all | bytes 163840 | tf_op jit(solution)/shard_map/all_to_all | solution.py:13
  124.7 0.8 copy.23
  125.5 7.1 %all-to-all-start.3 = ((bf16[16,320,16]{1,2,0:T(8,128)(2,1)}), bf16[16,320,16]{1,2,0:T(8,128)(2,1)S(1)}, u32[]{:S(2)}, u32[]{:S(2)}) async-start(bf16[16,320,16]{1,2,0:T(8,128)(2,1)} %bitcast.9), calls=%async_computation.3 | async-start | bytes 393216 | tf_op jit(solution)/shard_map/all_to_all | solution.py:34
  132.6 1.3 dynamic-slice.4
  134.6 8.3 %all-to-all-done.3 = bf16[16,320,16]{1,2,0:T(8,128)(2,1)S(1)} async-done(((bf16[16,320,16]{1,2,0:T(8,128)(2,1)}), bf16[16,320,16]{1,2,0:T(8,128)(2,1)S(1)}, u32[]{:S(2)}, u32[]{:S(2)}) %all-to-all-start.3) | async-done | bytes 163872 | tf_op jit(solution)/shard_map/all_to_all | solution.py:34
  142.9 15.1 %all_gather.10 = bf16[320,256]{0,1:T(8,128)(2,1)S(1)} all-gather(bf16[320,16]{0,1:T(8,128)(2,1)S(1)} %add_convert_fusion.1), channel_id=1, replica_groups=mesh['grp'=2,'kv'=16,'tp'=16] {'tp'}, dimensions={1}, use_global_device_ids=true | all-gather | bytes 174080 | tf_op jit(solution)/shard_map/all_gather | solution.py:133
  158.1 0.6 broadcast_in_dim.5
  158.7 3.9 %all-to-all-start.4 = ((f32[16,1,320]{2,1,0:T(1,128)}), f32[16,1,320]{2,1,0:T(1,128)S(1)}, u32[]{:S(2)}, u32[]{:S(2)}) async-start(f32[16,1,320]{2,1,0:T(1,128)} %broadcast_in_dim.5), calls=%async_computation.4 | async-start | bytes 49152 | tf_op jit(solution)/shard_map/all_to_all | solution.py:18
  162.6 0.4 convolution_convert_fusion
  163.1 0.4 convolution_convert_fusion.1
  163.6 32.1 %fusion = bf16[24,1792]{1,0:T(8,128)(2,1)S(1)} fusion(bf16[320,1792]{1,0:T(8,128)(2,1)S(1)} %pad_maximum_fusion), kind=kCustom, calls=%all-reduce-scatter | all-reduce-scatter fusion | flops 688129 | bytes 1234944
  195.7 2.3 collective-permute-start.1
  198.0 3.0 %collective-permute-start = (bf16[24,1792]{1,0:T(8,128)(2,1)S(1)}, bf16[24,1792]{1,0:T(8,128)(2,1)S(1)}, u32[]{:S(2)}, u32[]{:S(2)}) collective-permute-start(bf16[24,1792]{1,0:T(8,128)(2,1)S(1)} %fusion), channel_id=1, source_target_pairs={{0,16},{16,32},{32,48},{48,64},{64,80},{80,96},{96,112},{112,128},... | collective-permute-start | bytes 258056
  201.0 5.7 %collective-permute-start.2 = (bf16[12,1792]{1,0:T(8,128)(2,1)S(1)}, bf16[12,1792]{1,0:T(8,128)(2,1)S(1)}, u32[]{:S(2)}, u32[]{:S(2)}) collective-permute-start(bf16[12,1792]{1,0:T(8,128)(2,1)S(1)} %slice.50), channel_id=1, source_target_pairs={{0,48},{16,64},{32,80},{48,96},{64,112},{80,128},{96,144},{112,160... | collective-permute-start | bytes 129032
  206.8 1.1 collective-permute-done.2
  207.9 0.6 concatenate.40
  208.6 27.3 %all-gather = bf16[16,20,896]{2,1,0:T(8,128)(2,1)S(1)} all-gather(bf16[1,20,896]{2,1,0:T(8,128)(2,1)S(1)} %fusion.11), channel_id=1, replica_groups=mesh['grp'=2,'kv'=16,'tp'=16] {'kv'}, dimensions={0}, use_global_device_ids=true | all-gather | bytes 609280 | tf_op jit(solution)/shard_map/all_gather | solution.py:162
  236.0 0.3 convolution_convert_fusion.2
  236.5 31.5 %all_to_all.33 = bf16[16,320,16]{1,2,0:T(8,128)(2,1)S(1)} all-to-all(bf16[16,320,16]{1,2,0:T(8,128)(2,1)S(1)} %bitcast.43), channel_id=1, replica_groups=mesh['grp'=2,'kv'=16,'tp'=16] {'tp'}, dimensions={0} | all-to-all | bytes 327680 | tf_op jit(solution)/shard_map/all_to_all | solution.py:34
  268.1 0.6 add_convert_fusion
  (66 shorter events, 2.8 us)
Async XLA Ops:
  0.6 162.0 %copy-start = (bf16[256,896]{1,0:T(8,128)(2,1)S(1)}, bf16[256,896]{1,0:T(8,128)(2,1)}, u32[]{:S(2)}) copy-start(bf16[256,896]{1,0:T(8,128)(2,1)} %param.26) | copy-start | bytes 1376260
  0.6 67.3 %copy-start.6 = (bf16[256,128]{1,0:T(8,128)(2,1)S(1)}, bf16[256,128]{1,0:T(8,128)(2,1)}, u32[]{:S(2)}) copy-start(bf16[256,128]{1,0:T(8,128)(2,1)} %param.21) | copy-start | bytes 196612
  0.7 67.7 %copy-start.7 = (bf16[256,128]{1,0:T(8,128)(2,1)S(1)}, bf16[256,128]{1,0:T(8,128)(2,1)}, u32[]{:S(2)}) copy-start(bf16[256,128]{1,0:T(8,128)(2,1)} %param.18) | copy-start | bytes 196612
  57.8 18.4 %all-to-all-start.1 = ((f32[16,1,320]{2,1,0:T(1,128)}), f32[16,1,320]{2,1,0:T(1,128)S(1)}, u32[]{:S(2)}, u32[]{:S(2)}) async-start(f32[16,1,320]{2,1,0:T(1,128)} %broadcast_in_dim.4), calls=%async_computation.1 | async-start | bytes 49152 | tf_op jit(solution)/shard_map/all_to_all | solution.py:18
  68.0 13.1 %copy-start.9 = (s32[20]{0:T(128)S(1)}, s32[20]{0:T(128)}, u32[]{:S(2)}) copy-start(s32[20]{0:T(128)} %param.15) | copy-start | bytes 244
  68.0 13.1 %copy-start.10 = (bf16[128]{0:T(256)(128)(2,1)S(1)}, bf16[128]{0:T(256)(128)(2,1)}, u32[]{:S(2)}) copy-start(bf16[128]{0:T(256)(128)(2,1)} %param.22) | copy-start | bytes 772
  68.7 30.7 %copy-start.2 = (f32[20,1,128,128]{3,2,1,0:T(8,128)S(1)}, f32[20,1,128,128]{3,2,1,0:T(8,128)}, u32[]{:S(2)}) copy-start(f32[20,1,128,128]{3,2,1,0:T(8,128)} %param.16) | copy-start | bytes 3932164
  76.2 22.7 %all-to-all-start = ((bf16[16,20,512]{2,1,0:T(8,128)(2,1)}), bf16[16,20,512]{2,1,0:T(8,128)(2,1)S(1)}, u32[]{:S(2)}, u32[]{:S(2)}) async-start(bf16[16,20,512]{2,1,0:T(8,128)(2,1)} %pad_maximum_fusion.1), calls=%async_computation | async-start | bytes 786432 | tf_op jit(solution)/shard_map/all_to_all | solution.py:34
  99.8 25.7 %copy-start.1 = (f32[20,1,128,128]{3,2,1,0:T(8,128)}, f32[20,1,128,128]{3,2,1,0:T(8,128)S(1)}, u32[]{:S(2)}) copy-start(f32[20,1,128,128]{3,2,1,0:T(8,128)S(1)} %multiply_add_fusion) | copy-start | bytes 3932164
  99.8 24.7 %copy-start.5 = (bf16[128,256]{1,0:T(8,128)(2,1)S(1)}, bf16[128,256]{1,0:T(8,128)(2,1)}, u32[]{:S(2)}) copy-start(bf16[128,256]{1,0:T(8,128)(2,1)} %param.23) | copy-start | bytes 196612
  99.8 32.8 %copy-start.11 = (bf16[256]{0:T(256)(128)(2,1)S(1)}, bf16[256]{0:T(256)(128)(2,1)}, u32[]{:S(2)}) copy-start(bf16[256]{0:T(256)(128)(2,1)} %param.24) | copy-start | bytes 1540
  99.8 43.1 %copy-start.8 = (bf16[320,16]{0,1:T(8,128)(2,1)S(1)}, bf16[320,16]{0,1:T(8,128)(2,1)}, u32[]{:S(2)}) copy-start(bf16[320,16]{0,1:T(8,128)(2,1)} %param.14) | copy-start | bytes 30724
  124.7 38.4 %copy-start.3 = (bf16[256,896]{1,0:T(8,128)(2,1)S(1)}, bf16[256,896]{1,0:T(8,128)(2,1)}, u32[]{:S(2)}) copy-start(bf16[256,896]{1,0:T(8,128)(2,1)} %param.25) | copy-start | bytes 1376260
  125.5 17.3 %all-to-all-start.3 = ((bf16[16,320,16]{1,2,0:T(8,128)(2,1)}), bf16[16,320,16]{1,2,0:T(8,128)(2,1)S(1)}, u32[]{:S(2)}, u32[]{:S(2)}) async-start(bf16[16,320,16]{1,2,0:T(8,128)(2,1)} %bitcast.9), calls=%async_computation.3 | async-start | bytes 393216 | tf_op jit(solution)/shard_map/all_to_all | solution.py:34
  158.7 48.0 %all-to-all-start.4 = ((f32[16,1,320]{2,1,0:T(1,128)}), f32[16,1,320]{2,1,0:T(1,128)S(1)}, u32[]{:S(2)}, u32[]{:S(2)}) async-start(f32[16,1,320]{2,1,0:T(1,128)} %broadcast_in_dim.5), calls=%async_computation.4 | async-start | bytes 49152 | tf_op jit(solution)/shard_map/all_to_all | solution.py:18
  195.7 12.2 %collective-permute-start.1 = (bf16[24,1792]{1,0:T(8,128)(2,1)S(1)}, bf16[24,1792]{1,0:T(8,128)(2,1)S(1)}, u32[]{:S(2)}, u32[]{:S(2)}) collective-permute-start(bf16[24,1792]{1,0:T(8,128)(2,1)S(1)} %fusion), channel_id=1, source_target_pairs={{0,32},{16,48},{32,64},{48,80},{64,96},{80,112},{96,128},{112,144}... | collective-permute-start | bytes 258056
  198.0 9.9 %collective-permute-start = (bf16[24,1792]{1,0:T(8,128)(2,1)S(1)}, bf16[24,1792]{1,0:T(8,128)(2,1)S(1)}, u32[]{:S(2)}, u32[]{:S(2)}) collective-permute-start(bf16[24,1792]{1,0:T(8,128)(2,1)S(1)} %fusion), channel_id=1, source_target_pairs={{0,16},{16,32},{32,48},{48,64},{64,80},{80,96},{96,112},{112,128},... | collective-permute-start | bytes 258056
  201.0 6.9 %collective-permute-start.2 = (bf16[12,1792]{1,0:T(8,128)(2,1)S(1)}, bf16[12,1792]{1,0:T(8,128)(2,1)S(1)}, u32[]{:S(2)}, u32[]{:S(2)}) collective-permute-start(bf16[12,1792]{1,0:T(8,128)(2,1)S(1)} %slice.50), channel_id=1, source_target_pairs={{0,48},{16,64},{32,80},{48,96},{64,112},{80,128},{96,144},{112,160... | collective-permute-start | bytes 129032
  208.5 27.5 %copy-start.4 = (bf16[896,256]{1,0:T(8,128)(2,1)S(1)}, bf16[896,256]{1,0:T(8,128)(2,1)}, u32[]{:S(2)}) copy-start(bf16[896,256]{1,0:T(8,128)(2,1)} %param.27) | copy-start | bytes 1376260
